TPU v7x, 128 devices: a whole 4x4x4 slice. The times are simulated.
128 devices in a mesh: sp: 16 (over z, x), tp: 8 (over y, core).
Axes of the slice: x: 4, y: 4, z: 4, core: 2. Of those that a mesh axis runs over, the one named last changes fastest.
Arguments:
- tokens_in: bfloat16 [12288, 2048], P(('sp', 'tp')), may hold values from -300 to 300
- norm_gain: float32 [2048], replicated, may hold values from 0.1 to 1.9
- query_weight: bfloat16 [2048, 1024], P('sp', 'tp'), may hold values from -64 to 64
- key_weight: bfloat16 [2048, 512], P('sp', 'tp'), may hold values from -1 to 1
- value_weight: bfloat16 [2048, 512], P('sp', 'tp'), may hold values from -0.125 to 0.125
- pool_weight: bfloat16 [2048, 1024], P('sp', 'tp'), may hold values from -0.125 to 0.125
- sink_logit: float32 [16], P('tp'), may hold values from 1 to 5
- pool_gain: float32 [1024], P('tp'), may hold values from 0.1 to 1.9
- attention_out_weight: bfloat16 [1024, 2048], P('tp', 'sp'), may hold values from -0.125 to 0.125
- pool_out_weight: bfloat16 [1024, 2048], P('tp', 'sp'), may hold values from -0.1875 to 0.1875
Outputs:
- mixed_out: bfloat16 [12288, 2048], P(('sp', 'tp'))
All inputs are finite; a program needn't handle non-finite values.
Results may differ from a plain program's by a relative error of at most 0.014.
Values may be sent and summed in bfloat16 or wider, within the bound.
A program may use at most 64 MiB of HBM per device.

v0:
```python
import jax
import jax.numpy as jnp
from jax import lax
from jax.sharding import PartitionSpec as P

HEAD_DIM = 64
POOL_CH = 256
POOL_GROUPS = 4
WINDOW = 128
EPS = 1e-06
SHORT_REACHES = (8, 32)


def sent_together(arrays, axis, dim, along):
    ends, at = ([], 0)
    for a in arrays[:-1]:
        at += a.shape[along]
        ends.append(at)
    both = jnp.concatenate(arrays, axis=along)
    return tuple(jnp.split(lax.all_gather(both, axis, axis=dim, tiled=True), ends, axis=along))


def passed_along(block, axis, distance):
    devices = range(lax.axis_size(axis))
    route = [(i - distance, i) for i in devices if i - distance in devices]
    return lax.ppermute(block, axis, route)


def from_everyone(x, axis):
    copies = jnp.broadcast_to(x, (lax.axis_size(axis), *x.shape))
    return lax.all_to_all(copies, axis, split_axis=0, concat_axis=0, tiled=True)


def in_order(parts, dim):
    parts = jnp.moveaxis(parts, 0, dim)
    shape = parts.shape
    return parts.reshape(*shape[:dim], shape[dim] * shape[dim + 1], *shape[dim + 2 :])


def gathered_copies(x, axis, dim):
    parts = from_everyone(x, axis)
    return in_order(parts, dim)


def local(
    tokens_in,
    norm_gain,
    query_weight,
    key_weight,
    value_weight,
    pool_weight,
    sink_logit,
    pool_gain,
    attention_out_weight,
    pool_out_weight,
):
    widened = tokens_in.astype(jnp.float32)
    inverse = lax.rsqrt(jnp.mean(widened * widened, axis=1, keepdims=True) + EPS)
    normed = (widened * inverse * norm_gain).astype(jnp.bfloat16)
    all_rows = lax.all_gather(normed, "tp", axis=0, tiled=True)
    pieces = sent_together((query_weight, key_weight, value_weight, pool_weight), "sp", 0, 1)
    projected = tuple(
        (
            jnp.dot(all_rows, weight_piece, preferred_element_type=jnp.float32)
            for weight_piece in pieces
        )
    )
    query_rows, key_rows, value_rows, pool_rows = [
        projection.astype(jnp.bfloat16) for projection in projected
    ]
    seq_len = query_rows.shape[0]
    offset = lax.axis_index("sp") * seq_len
    halo_keys, halo_values, halo_pool = passed_along(
        (
            key_rows[seq_len - WINDOW :],
            value_rows[seq_len - WINDOW :],
            pool_rows[seq_len - WINDOW :],
        ),
        "sp",
        1,
    )
    kv_local = key_rows.shape[1] // HEAD_DIM
    heads_local = query_rows.shape[1] // HEAD_DIM
    group = heads_local // kv_local
    blocks = seq_len // WINDOW
    key_ext = jnp.concatenate([halo_keys, key_rows], axis=0).reshape(
        blocks + 1, WINDOW, kv_local, HEAD_DIM
    )
    value_ext = jnp.concatenate([halo_values, value_rows], axis=0).reshape(
        blocks + 1, WINDOW, kv_local, HEAD_DIM
    )
    key_pairs = jnp.concatenate([key_ext[:-1], key_ext[1:]], axis=1)
    value_pairs = jnp.concatenate([value_ext[:-1], value_ext[1:]], axis=1)
    query_blocks = query_rows.reshape(blocks, WINDOW, kv_local, group, HEAD_DIM)
    scores = jnp.einsum(
        "nqhgd,nkhd->nhgqk", query_blocks, key_pairs, preferred_element_type=jnp.float32
    ) * HEAD_DIM ** (-0.5)
    shape_mask = (blocks, WINDOW, 2 * WINDOW)
    q_index = lax.broadcasted_iota(jnp.int32, shape_mask, 1)
    k_index = lax.broadcasted_iota(jnp.int32, shape_mask, 2)
    block_index = lax.broadcasted_iota(jnp.int32, shape_mask, 0)
    distance = q_index + WINDOW - k_index
    key_position = offset + block_index * WINDOW + k_index - WINDOW
    allowed = (distance >= 0) & (distance < WINDOW) & (key_position >= 0)
    scores = jnp.where(allowed[:, None, None], scores, -jnp.inf)
    sinks = sink_logit.reshape(1, kv_local, group, 1, 1)
    peak = jnp.maximum(jnp.max(scores, axis=-1, keepdims=True), sinks)
    expo = jnp.exp(scores - peak)
    denom = jnp.sum(expo, axis=-1, keepdims=True) + jnp.exp(sinks - peak)
    probs = (expo / denom).astype(jnp.bfloat16)
    attended = jnp.einsum(
        "nhgqk,nkhd->nqhgd", probs, value_pairs, preferred_element_type=jnp.float32
    )
    attended = attended.astype(jnp.bfloat16).reshape(seq_len, heads_local * HEAD_DIM)
    pool_values = pool_rows.astype(jnp.float32)
    channels = pool_rows.shape[1]
    pool_ext = jnp.concatenate([halo_pool.astype(jnp.float32), pool_values], axis=0)
    running = jnp.concatenate(
        [jnp.zeros((1, channels), jnp.float32), jnp.cumsum(pool_ext, axis=0)], axis=0
    )
    group_id = lax.axis_index("tp") * channels // POOL_CH
    reach = jnp.where(
        group_id == 0, SHORT_REACHES[0], jnp.where(group_id == 1, SHORT_REACHES[1], WINDOW)
    ).astype(jnp.int32)
    upper = running[WINDOW + 1 :]
    lower = lax.dynamic_slice_in_dim(running, WINDOW + 1 - reach, seq_len, 0)
    position = offset + lax.broadcasted_iota(jnp.int32, (seq_len,), 0)
    counted = jnp.minimum(position + 1, reach).astype(jnp.float32)[:, None]
    windowed = (upper - lower) / counted
    own_sums = upper - running[WINDOW]
    device_total = own_sums[seq_len - 1]
    totals = gathered_copies(device_total[None, :], "sp", 0)
    earlier_rows = lax.broadcasted_iota(jnp.int32, (totals.shape[0], 1), 0) < lax.axis_index("sp")
    before = jnp.sum(jnp.where(earlier_rows, totals, 0.0), axis=0)
    cumulative = (before[None, :] + own_sums) / (position + 1).astype(jnp.float32)[:, None]
    pooled = jnp.where(group_id == POOL_GROUPS - 1, cumulative, windowed)
    pool_mixed = ((pooled - pool_values) * pool_gain).astype(jnp.bfloat16)
    out_attend, out_pool = sent_together((attention_out_weight, pool_out_weight), "sp", 1, 0)
    return lax.psum_scatter(
        (
            jnp.dot(attended, out_attend, preferred_element_type=jnp.float32)
            + jnp.dot(pool_mixed, out_pool, preferred_element_type=jnp.float32)
        ).astype(jnp.bfloat16),
        "tp",
        scatter_dimension=0,
        tiled=True,
    )


def solution(mesh):
    in_specs = (
        P(("sp", "tp"), None),
        P(),
        P("sp", "tp"),
        P("sp", "tp"),
        P("sp", "tp"),
        P("sp", "tp"),
        P("tp"),
        P("tp"),
        P("tp", "sp"),
        P("tp", "sp"),
    )
    out_specs = P(("sp", "tp"), None)
    return jax.shard_map(local, mesh=mesh, in_specs=in_specs, out_specs=out_specs, check_vma=False)
```

profile of v0, /device:TPU:0, one launch (start us, length us, event | category | flops | bytes accessed | tf_op | source)
XLA Modules:
  0.0 182.7 jit_solution(4462187103619193170)
XLA Ops:
  6.5 0.0 all-gather.6.cloned.1.call-start
  6.5 0.8 copy.33
  7.4 0.8 copy.34
  8.2 1.5 pad_maximum_fusion.3
  9.7 0.0 all-gather.6.cloned.1.call-update
  9.7 0.0 all-gather.4.cloned.1.call-start
  9.8 1.2 fusion.2
  11.0 1.9 %fusion.4 = bf16[96,2048]{1,0:T(8,128)(2,1)} fusion(bf16[96,2048]{1,0:T(8,128)(2,1)} %param.10, f32[2048]{0:T(1024)} %param.11, f32[96]{0:T(128)S(1)} %add_rsqrt_fusion), kind=kLoop, calls=%fused_computation.15 | loop fusion | flops 786432 | bytes 795008 | tf_op jit(solution)/shard_map/convert_element_type | solution.py:59
  12.9 0.0 all-gather.4.cloned.1.call-update
  12.9 0.0 all-gather.8.cloned.1.call-start
  13.0 0.0 copy-done.8
  13.0 0.0 copy-done.9
  13.0 0.6 pad_maximum_fusion.4
  13.6 0.0 all-gather.8.cloned.1.call-update
  13.8 1.0 fusion.8
  14.7 41.5 %all-gather.6.cloned.1.call-done = bf16[2048,384]{1,0:T(8,128)(2,1)} async-done(((bf16[128,384]{1,0:T(8,128)(2,1)}), bf16[2048,384]{1,0:T(8,128)(2,1)}) %all-gather.6.cloned.1.call-update) | async-done | bytes 1572880 | tf_op jit(solution)/shard_map/all_gather | solution.py:20
  56.2 28.7 %all-gather.4.cloned.1.call-done = bf16[768,2048]{1,0:T(8,128)(2,1)} async-done(((bf16[96,2048]{1,0:T(8,128)(2,1)}), bf16[768,2048]{1,0:T(8,128)(2,1)}) %all-gather.4.cloned.1.call-update) | async-done | bytes 3145744 | tf_op jit(solution)/shard_map/all_gather | solution.py:60
  84.9 3.2 %convolution_convert_fusion.3 = bf16[768,64]{0,1:T(8,128)(2,1)S(1)} fusion(bf16[768,2048]{1,0:T(8,128)(2,1)} %all-gather.4.cloned.1.call-done, bf16[2048,384]{1,0:T(8,128)(2,1)} %all-gather.6.cloned.1.call-done), kind=kOutput, calls=%fused_computation.9 | convolution fusion | flops 201375744 | bytes 3768320 | tf_op jit(solution)/shard_map/dot_general | solution.py:64
  88.1 0.6 slice.62
  88.7 0.0 copy-done.6
  88.8 0.1 slice.53
  88.9 0.0 copy-done
  88.9 2.2 %convolution_convert_fusion.4 = bf16[768,64]{0,1:T(8,128)(2,1)S(1)} fusion(bf16[768,2048]{1,0:T(8,128)(2,1)S(1)} %copy-done, bf16[2048,384]{1,0:T(8,128)(2,1)} %all-gather.6.cloned.1.call-done), kind=kOutput, calls=%fused_computation.10 | convolution fusion | flops 201375744 | bytes 3768320 | tf_op jit(solution)/shard_map/dot_general | solution.py:64
  91.1 0.6 slice.61
  91.8 0.1 slice.49
  91.9 4.0 %collective-permute-start.1 = (bf16[128,64]{0,1:T(8,128)(2,1)}, bf16[128,64]{0,1:T(8,128)(2,1)}, u32[]{:S(2)}, u32[]{:S(2)}) collective-permute-start(bf16[128,64]{0,1:T(8,128)(2,1)} %slice.62), channel_id=1, source_target_pairs={{0,8},{8,16},{16,24},{24,32},{32,40},{40,48},{48,56},{56,64},{64,7... | collective-permute-start | bytes 49160 | tf_op jit(solution)/shard_map/ppermute | solution.py:26
  95.9 0.6 copy.38
  96.5 3.4 %collective-permute-start = (bf16[128,64]{0,1:T(8,128)(2,1)}, bf16[128,64]{0,1:T(8,128)(2,1)}, u32[]{:S(2)}, u32[]{:S(2)}) collective-permute-start(bf16[128,64]{0,1:T(8,128)(2,1)} %slice.61), channel_id=1, source_target_pairs={{0,8},{8,16},{16,24},{24,32},{32,40},{40,48},{48,56},{56,64},{64,7... | collective-permute-start | bytes 49160 | tf_op jit(solution)/shard_map/ppermute | solution.py:26
  99.9 0.0 copy-done.4
  99.9 0.6 copy.36
  100.6 2.0 %fusion.45 = (f32[768,128]{1,0:T(8,128)S(1)}, bf16[768,128]{1,0:T(8,128)(2,1)S(1)}) fusion(bf16[768,2048]{1,0:T(8,128)(2,1)S(1)} %copy-done, bf16[2048,384]{1,0:T(8,128)(2,1)} %all-gather.6.cloned.1.call-done), kind=kOutput, calls=%fused_computation.79 | convolution fusion | flops 402849792 | bytes 4259840 | tf_op jit(solution)/shard_map/dot_general | solution.py:64
  102.6 0.7 copy-done.1
  103.2 0.6 slice.63
  103.8 3.1 %collective-permute-start.2 = (bf16[128,128]{1,0:T(8,128)(2,1)}, bf16[128,128]{1,0:T(8,128)(2,1)}, u32[]{:S(2)}, u32[]{:S(2)}) collective-permute-start(bf16[128,128]{1,0:T(8,128)(2,1)} %slice.63), channel_id=1, source_target_pairs={{0,8},{8,16},{16,24},{24,32},{32,40},{40,48},{48,56},{56,64},{64,7... | collective-permute-start | bytes 98312 | tf_op jit(solution)/shard_map/ppermute | solution.py:26
  106.9 2.7 %convolution_convert_fusion.1 = bf16[768,128]{1,0:T(8,128)(2,1)} fusion(bf16[768,2048]{1,0:T(8,128)(2,1)S(1)} %copy-done, bf16[2048,384]{1,0:T(8,128)(2,1)} %all-gather.6.cloned.1.call-done), kind=kOutput, calls=%fused_computation.6 | convolution fusion | flops 402751488 | bytes 3866624 | tf_op jit(solution)/shard_map/dot_general | solution.py:64
  109.6 1.1 reshape.121
  110.7 0.0 collective-permute-done.1
  110.8 0.9 pad_maximum_fusion.1
  111.7 0.0 copy-start.10
  111.7 0.1 slice.52
  111.8 1.5 fusion.44
  113.3 0.1 broadcast_maximum_fusion
  113.4 0.2 fusion
  113.7 0.1 exponential_add_fusion
  113.7 0.0 collective-permute-done
  113.8 0.7 pad_maximum_fusion.2
  114.5 0.1 slice.48
  114.7 0.4 fusion.1
  115.1 0.1 copy.42
  115.2 0.0 collective-permute-done.2
  115.2 0.8 convert_element_type.66
  116.0 0.3 fusion.17
  116.4 0.1 copy.44
  116.5 0.6 broadcast_in_dim.40
  117.1 6.1 %all-to-all-start = ((f32[16,1,128]{2,1,0:T(1,128)}), f32[16,1,128]{2,1,0:T(1,128)S(1)}, u32[]{:S(2)}, u32[]{:S(2)}) async-start(f32[16,1,128]{2,1,0:T(1,128)} %broadcast_in_dim.40), calls=%async_computation | async-start | bytes 16384 | tf_op jit(solution)/shard_map/all_to_all | solution.py:31
  123.3 0.0 reduce-scatter.2.cloned.1.call-start
  123.3 7.0 %all-gather.8.cloned.1.call-done = bf16[256,2048]{1,0:T(8,128)(2,1)} async-done(((bf16[256,128]{1,0:T(8,128)(2,1)}), bf16[256,2048]{1,0:T(8,128)(2,1)}) %all-gather.8.cloned.1.call-update) | async-done | bytes 1048592 | tf_op jit(solution)/shard_map/all_gather | solution.py:20
  130.3 4.8 %fusion.12 = f32[768,2048]{1,0:T(8,128)} fusion(bf16[256,2048]{1,0:T(8,128)(2,1)} %all-gather.8.cloned.1.call-done, bf16[16,8,6,128]{3,2,1,0:T(8,128)(2,1)S(1)} %bitcast.62), kind=kOutput, calls=%fused_computation.25 | convolution fusion | flops 402653184 | bytes 7012352 | tf_op jit(solution)/shard_map/dot_general | solution.py:141
  135.1 0.0 all-to-all-done
  135.1 0.1 select_reduce_fusion
  135.2 0.0 copy-done.2
  135.2 5.6 %add_convert_fusion = bf16[768,2048]{1,0:T(8,128)(2,1)} fusion(f32[768,2048]{1,0:T(8,128)} %fusion.12, bf16[256,2048]{1,0:T(8,128)(2,1)S(1)} %copy-done.3, s32[]{:T(128)S(6)} %select_n.38, f32[896,128]{1,0:T(8,128)S(1)} %bitcast.60, f32[768,128]{1,0:T(8,128)S(1)} %slice_subtract_fusion, f32[128]{0:T(128)S(1)} %copy-done.11, f32[768]{0:T(1024)S(1)} %get-tuple-element.9, ...), kind=kOutput, calls=%fused_computation | convolution fusion | flops 406683648 | bytes 11412485 | tf_op jit(solution)/shard_map/dot_general | solution.py:142
  140.8 0.0 reduce-scatter.2.cloned.1.call-update
  140.8 35.3 %reduce-scatter.2.cloned.1.call-done = bf16[96,2048]{1,0:T(8,128)(2,1)} async-done(((bf16[768,2048]{1,0:T(8,128)(2,1)}), bf16[96,2048]{1,0:T(8,128)(2,1)}) %reduce-scatter.2.cloned.1.call-update) | async-done | bytes 393232 | tf_op jit(solution)/shard_map/reduce_scatter | solution.py:139
  (30 shorter events, 0.2 us)
Async XLA Ops:
  6.5 6.4 %copy-start.8 = (bf16[128,128]{1,0:T(8,128)(2,1)S(1)}, bf16[128,128]{1,0:T(8,128)(2,1)}, u32[]{:S(2)}) copy-start(bf16[128,128]{1,0:T(8,128)(2,1)} %param.19) | copy-start | bytes 98308
  6.5 6.5 %copy-start.9 = (bf16[128,128]{1,0:T(8,128)(2,1)S(1)}, bf16[128,128]{1,0:T(8,128)(2,1)}, u32[]{:S(2)}) copy-start(bf16[128,128]{1,0:T(8,128)(2,1)} %param.18) | copy-start | bytes 98308
  6.5 49.7 %all-gather.6.cloned.1.call-start = ((), (), s32[]{:S(2)}) async-start(), calls=%async_computation.3 | async-start | bytes 1671168 | tf_op jit(solution)/shard_map/all_gather | solution.py:20
  9.7 75.1 %all-gather.4.cloned.1.call-start = ((), (), s32[]{:S(2)}) async-start(), calls=%async_computation.2 | async-start | bytes 3538944 | tf_op jit(solution)/shard_map/all_gather | solution.py:60
  12.9 117.4 %all-gather.8.cloned.1.call-start = ((), (), s32[]{:S(2)}) async-start(), calls=%async_computation.4 | async-start | bytes 1114112 | tf_op jit(solution)/shard_map/all_gather | solution.py:20
  84.9 4.0 %copy-start = (bf16[768,2048]{1,0:T(8,128)(2,1)S(1)}, bf16[768,2048]{1,0:T(8,128)(2,1)}, u32[]{:S(2)}) copy-start(bf16[768,2048]{1,0:T(8,128)(2,1)} %all-gather.4.cloned.1.call-done) | copy-start | bytes 9437188
  88.1 0.7 copy-start.6
  91.1 8.8 %copy-start.4 = (bf16[768,64]{0,1:T(8,128)(2,1)}, bf16[768,64]{0,1:T(8,128)(2,1)S(1)}, u32[]{:S(2)}) copy-start(bf16[768,64]{0,1:T(8,128)(2,1)S(1)} %convolution_convert_fusion.4) | copy-start | bytes 294916
  91.9 18.8 %collective-permute-start.1 = (bf16[128,64]{0,1:T(8,128)(2,1)}, bf16[128,64]{0,1:T(8,128)(2,1)}, u32[]{:S(2)}, u32[]{:S(2)}) collective-permute-start(bf16[128,64]{0,1:T(8,128)(2,1)} %slice.62), channel_id=1, source_target_pairs={{0,8},{8,16},{16,24},{24,32},{32,40},{40,48},{48,56},{56,64},{64,7... | collective-permute-start | bytes 49160 | tf_op jit(solution)/shard_map/ppermute | solution.py:26
  96.5 17.2 %collective-permute-start = (bf16[128,64]{0,1:T(8,128)(2,1)}, bf16[128,64]{0,1:T(8,128)(2,1)}, u32[]{:S(2)}, u32[]{:S(2)}) collective-permute-start(bf16[128,64]{0,1:T(8,128)(2,1)} %slice.61), channel_id=1, source_target_pairs={{0,8},{8,16},{16,24},{24,32},{32,40},{40,48},{48,56},{56,64},{64,7... | collective-permute-start | bytes 49160 | tf_op jit(solution)/shard_map/ppermute | solution.py:26
  102.6 0.7 copy-start.1
  103.8 11.4 %collective-permute-start.2 = (bf16[128,128]{1,0:T(8,128)(2,1)}, bf16[128,128]{1,0:T(8,128)(2,1)}, u32[]{:S(2)}, u32[]{:S(2)}) collective-permute-start(bf16[128,128]{1,0:T(8,128)(2,1)} %slice.63), channel_id=1, source_target_pairs={{0,8},{8,16},{16,24},{24,32},{32,40},{40,48},{48,56},{56,64},{64,7... | collective-permute-start | bytes 98312 | tf_op jit(solution)/shard_map/ppermute | solution.py:26
  111.7 1.7 copy-start.10
  111.8 1.9 %copy-start.5 = (bf16[768,64]{0,1:T(8,128)(2,1)S(1)}, bf16[768,64]{0,1:T(8,128)(2,1)}, u32[]{:S(2)}) copy-start(bf16[768,64]{0,1:T(8,128)(2,1)} %copy-done.4) | copy-start | bytes 294916
  113.3 1.3 copy-start.7
  117.1 18.0 %all-to-all-start = ((f32[16,1,128]{2,1,0:T(1,128)}), f32[16,1,128]{2,1,0:T(1,128)S(1)}, u32[]{:S(2)}, u32[]{:S(2)}) async-start(f32[16,1,128]{2,1,0:T(1,128)} %broadcast_in_dim.40), calls=%async_computation | async-start | bytes 16384 | tf_op jit(solution)/shard_map/all_to_all | solution.py:31
  123.3 52.8 %reduce-scatter.2.cloned.1.call-start = ((), (), s32[]{:S(2)}) async-start(), calls=%async_computation.5 | async-start | bytes 3538944 | tf_op jit(solution)/shard_map/reduce_scatter | solution.py:139
  130.3 4.9 %copy-start.2 = (bf16[768,128]{1,0:T(8,128)(2,1)S(1)}, bf16[768,128]{1,0:T(8,128)(2,1)}, u32[]{:S(2)}) copy-start(bf16[768,128]{1,0:T(8,128)(2,1)} %copy-done.1) | copy-start | bytes 589828
  130.3 4.9 %copy-start.3 = (bf16[256,2048]{1,0:T(8,128)(2,1)S(1)}, bf16[256,2048]{1,0:T(8,128)(2,1)}, u32[]{:S(2)}) copy-start(bf16[256,2048]{1,0:T(8,128)(2,1)} %all-gather.8.cloned.1.call-done) | copy-start | bytes 3145732
  130.3 4.9 %copy-start.11 = (f32[128]{0:T(128)S(1)}, f32[128]{0:T(128)}, u32[]{:S(2)}) copy-start(f32[128]{0:T(128)} %param.17) | copy-start | bytes 1540
Sparse Core Ops, SparseCore 0:
  9.9 46.2 all-gather.5
  57.9 26.9 all-gather.3
  87.0 43.2 all-gather.7
  141.0 35.1 reduce-scatter.1
where the time goes:
time: 183 us
  waiting for transfers between devices  112 us (61%)
  matrix products  22.4 us (12%)
  starting transfers between devices  16.7 us (9%)
  between operations  13.5 us (7%)
  other arithmetic  9.51 us (5%)
  local copies, waits for them, and re-layouts  8.08 us (4%)
    all_gather x2, waiting for transfers between devices, sent_together(): lax.all_gather(both, axis, axis=dim, tiled=True)  48.4 us
    reduce_scatter x1, waiting for transfers between devices, local(): lax.psum_scatter((jnp.dot(attended, out_attend, preferred_element_type=jn...  35.3 us
    all_gather x1, waiting for transfers between devices, local(): all_rows = lax.all_gather(normed, 'tp', axis=0, tiled=True)  28.7 us
    ppermute x3, starting transfers between devices, passed_along(): return lax.ppermute(block, axis, route)  10.4 us
    dot_general x4, matrix products, local(): jnp.dot(all_rows, weight_piece, preferred_element_type=jnp.float32)  10.1 us
    all_to_all x1, starting transfers between devices, from_everyone(): return lax.all_to_all(copies, axis, split_axis=0, concat_axis=0, tiled=True)  6.14 us
    dot_general x1, matrix products, local(): jnp.dot(pool_mixed, out_pool, preferred_element_type=jnp.float32)  5.6 us
    dot_general x1, matrix products, local(): jnp.dot(attended, out_attend, preferred_element_type=jnp.float32)  4.8 us
  transfers between devices with their start and end apart: 8, of which 4 were waited for; matrix products, arithmetic and copies ran while one was open for 17% of the time, Pallas kernels for 0%

commit v1 on v0

--- a/solution.py
+++ b/solution.py
@@ -2,6 +2,7 @@
 import jax.numpy as jnp
 from jax import lax
 from jax.sharding import PartitionSpec as P
+from jax.lax import all_to_all, axis_size
 
 HEAD_DIM = 64
 POOL_CH = 256
@@ -57,7 +58,7 @@
     widened = tokens_in.astype(jnp.float32)
     inverse = lax.rsqrt(jnp.mean(widened * widened, axis=1, keepdims=True) + EPS)
     normed = (widened * inverse * norm_gain).astype(jnp.bfloat16)
-    all_rows = lax.all_gather(normed, "tp", axis=0, tiled=True)
+    all_rows = jnp.concatenate(all_to_all(jnp.stack([normed] * axis_size("tp"), 0), "tp", 0, 0), 0)
     pieces = sent_together((query_weight, key_weight, value_weight, pool_weight), "sp", 0, 1)
     projected = tuple(
         (

time: 183 us -> 154 us (0.84)
  waiting for transfers between devices: 112 us -> 77.2 us
  starting transfers between devices: 16.7 us -> 22.5 us
  local copies, waits for them, and re-layouts: 8.08 us -> 10.1 us
    all_gather x2, waiting for transfers between devices: 48.4 us -> 5.16 us  [sent_together(): lax.all_gather(both, axis, axis=dim, tiled=True)]
    all_to_all x0 -> x1, waiting for transfers between devices: none -> 36.6 us  [local(): all_to_all(jnp.stack([normed] * axis_size('tp'), 0), 'tp', 0, 0)]
    all_gather x1 -> x0, waiting for transfers between devices: 28.7 us -> none  [local(): all_rows = lax.all_gather(normed, 'tp', axis=0, tiled=True)]
    all_to_all x0 -> x1, starting transfers between devices: none -> 4.71 us  [local(): all_to_all(jnp.stack([normed] * axis_size('tp'), 0), 'tp', 0, 0)]
    another operation x3 -> x4, local copies, waits for them, and re-layouts: 1.2 us -> 3.23 us  [the longest x1 2.03 us: local(): jnp.stack([normed] * axis_size('tp'), 0)]
  transfers between devices with their start and end apart: 8 -> 8, of which waited for: 4 -> 3; matrix products, arithmetic and copies ran while one was open for 17% -> 20% of each run, Pallas kernels for 0% -> 0%
where the time goes in v1:
time: 154 us; the launch traced here: 153 us
  waiting for transfers between devices  77.2 us (50%)
  starting transfers between devices  22.5 us (15%)
  matrix products  21.3 us (14%)
  between operations  13.4 us (9%)
  local copies, waits for them, and re-layouts  10.1 us (7%)
  other arithmetic  8.76 us (6%)
    all_to_all x1, waiting for transfers between devices, local(): all_to_all(jnp.stack([normed] * axis_size('tp'), 0), 'tp', 0, 0)  36.6 us
    reduce_scatter x1, waiting for transfers between devices, local(): lax.psum_scatter((jnp.dot(attended, out_attend, preferred_element_type=jn...  35.3 us
    ppermute x3, starting transfers between devices, passed_along(): return lax.ppermute(block, axis, route)  10.5 us
    dot_general x4, matrix products, local(): jnp.dot(all_rows, weight_piece, preferred_element_type=jnp.float32)  9.02 us
    all_to_all x1, starting transfers between devices, from_everyone(): return lax.all_to_all(copies, axis, split_axis=0, concat_axis=0, tiled=True)  7.22 us
    dot_general x1, matrix products, local(): jnp.dot(pool_mixed, out_pool, preferred_element_type=jnp.float32)  5.57 us
    all_gather x2, waiting for transfers between devices, sent_together(): lax.all_gather(both, axis, axis=dim, tiled=True)  5.16 us
    dot_general x1, matrix products, local(): jnp.dot(attended, out_attend, preferred_element_type=jnp.float32)  4.81 us
  transfers between devices with their start and end apart: 8, of which 3 were waited for; matrix products, arithmetic and copies ran while one was open for 20% of the time, Pallas kernels for 0%

profile of v1, /device:TPU:0, one launch (start us, length us, event | category | flops | bytes accessed | tf_op | source)
XLA Modules:
  0.0 153.3 jit_solution(9261544442912208577)
XLA Ops:
  6.5 0.8 copy.33
  7.4 0.8 copy.34
  8.2 1.5 pad_maximum_fusion.3
  9.7 0.0 all-gather.3.cloned.1.call-update
  9.7 1.2 fusion.2
  10.9 1.2 fusion.4
  12.1 2.0 %stack.2 = bf16[8,96,2048]{2,1,0:T(8,128)(2,1)} broadcast(bf16[96,2048]{1,0:T(8,128)(2,1)S(1)} %fusion.4), dimensions={1,2} | broadcast | bytes 3538944 | tf_op jit(solution)/shard_map/stack | solution.py:61
  14.1 4.7 %all-to-all-start = ((bf16[8,96,2048]{2,1,0:T(8,128)(2,1)}), bf16[8,96,2048]{2,1,0:T(8,128)(2,1)S(1)}, u32[]{:S(2)}, u32[]{:S(2)}) async-start(bf16[8,96,2048]{2,1,0:T(8,128)(2,1)} %stack.2), calls=%async_computation | async-start | bytes 6291456 | tf_op jit(solution)/shard_map/all_to_all | solution.py:61
  18.9 0.0 all-gather.5.cloned.1.call-start
  18.9 0.0 copy-done.7
  18.9 0.0 copy-done.8
  18.9 0.6 pad_maximum_fusion.4
  19.5 0.0 all-gather.5.cloned.1.call-update
  19.7 1.0 fusion.8
  20.7 36.6 %all-to-all-done = bf16[8,96,2048]{2,1,0:T(8,128)(2,1)S(1)} async-done(((bf16[8,96,2048]{2,1,0:T(8,128)(2,1)}), bf16[8,96,2048]{2,1,0:T(8,128)(2,1)S(1)}, u32[]{:S(2)}, u32[]{:S(2)}) %all-to-all-start) | async-done | bytes 3145760 | tf_op jit(solution)/shard_map/all_to_all | solution.py:61
  57.3 2.1 %convolution_convert_fusion.3 = bf16[768,64]{0,1:T(8,128)(2,1)S(1)} fusion(bf16[768,2048]{1,0:T(8,128)(2,1)S(1)} %bitcast.59, bf16[2048,384]{1,0:T(8,128)(2,1)} %all-gather.3.cloned.1.call-done), kind=kOutput, calls=%fused_computation.9 | convolution fusion | flops 201375744 | bytes 3768320 | tf_op jit(solution)/shard_map/dot_general | solution.py:65
  59.4 0.6 slice.62
  60.0 0.0 copy-done.5
  60.0 0.1 slice.53
  60.2 2.2 %convolution_convert_fusion.4 = bf16[768,64]{0,1:T(8,128)(2,1)S(1)} fusion(bf16[768,2048]{1,0:T(8,128)(2,1)S(1)} %bitcast.60, bf16[2048,384]{1,0:T(8,128)(2,1)} %all-gather.3.cloned.1.call-done), kind=kOutput, calls=%fused_computation.10 | convolution fusion | flops 201375744 | bytes 3768320 | tf_op jit(solution)/shard_map/dot_general | solution.py:65
  62.4 0.6 slice.61
  63.0 0.1 slice.49
  63.2 4.0 %collective-permute-start.1 = (bf16[128,64]{0,1:T(8,128)(2,1)}, bf16[128,64]{0,1:T(8,128)(2,1)}, u32[]{:S(2)}, u32[]{:S(2)}) collective-permute-start(bf16[128,64]{0,1:T(8,128)(2,1)} %slice.62), channel_id=1, source_target_pairs={{0,8},{8,16},{16,24},{24,32},{32,40},{40,48},{48,56},{56,64},{64,7... | collective-permute-start | bytes 49160 | tf_op jit(solution)/shard_map/ppermute | solution.py:27
  67.1 0.6 copy.38
  67.8 3.4 %collective-permute-start = (bf16[128,64]{0,1:T(8,128)(2,1)}, bf16[128,64]{0,1:T(8,128)(2,1)}, u32[]{:S(2)}, u32[]{:S(2)}) collective-permute-start(bf16[128,64]{0,1:T(8,128)(2,1)} %slice.61), channel_id=1, source_target_pairs={{0,8},{8,16},{16,24},{24,32},{32,40},{40,48},{48,56},{56,64},{64,7... | collective-permute-start | bytes 49160 | tf_op jit(solution)/shard_map/ppermute | solution.py:27
  71.2 0.0 copy-done.3
  71.2 0.6 copy.36
  71.8 2.0 %fusion.45 = (f32[768,128]{1,0:T(8,128)S(1)}, bf16[768,128]{1,0:T(8,128)(2,1)S(1)}) fusion(bf16[768,2048]{1,0:T(8,128)(2,1)S(1)} %bitcast.61, bf16[2048,384]{1,0:T(8,128)(2,1)} %all-gather.3.cloned.1.call-done), kind=kOutput, calls=%fused_computation.79 | convolution fusion | flops 402849792 | bytes 4259840 | tf_op jit(solution)/shard_map/dot_general | solution.py:65
  73.8 0.0 copy-start
  73.9 0.7 copy-done
  74.5 0.6 slice.63
  75.1 3.1 %collective-permute-start.2 = (bf16[128,128]{1,0:T(8,128)(2,1)}, bf16[128,128]{1,0:T(8,128)(2,1)}, u32[]{:S(2)}, u32[]{:S(2)}) collective-permute-start(bf16[128,128]{1,0:T(8,128)(2,1)} %slice.63), channel_id=1, source_target_pairs={{0,8},{8,16},{16,24},{24,32},{32,40},{40,48},{48,56},{56,64},{64,7... | collective-permute-start | bytes 98312 | tf_op jit(solution)/shard_map/ppermute | solution.py:27
  78.2 2.7 %convolution_convert_fusion.1 = bf16[768,128]{1,0:T(8,128)(2,1)} fusion(bf16[768,2048]{1,0:T(8,128)(2,1)S(1)} %bitcast.62, bf16[2048,384]{1,0:T(8,128)(2,1)} %all-gather.3.cloned.1.call-done), kind=kOutput, calls=%fused_computation.6 | convolution fusion | flops 402751488 | bytes 3866624 | tf_op jit(solution)/shard_map/dot_general | solution.py:65
  80.9 1.1 reshape.127
  82.0 0.0 collective-permute-done.1
  82.1 0.9 pad_maximum_fusion.1
  83.0 0.0 copy-start.9
  83.0 0.1 slice.52
  83.1 0.0 copy-start.4
  83.1 1.5 fusion.44
  84.6 0.1 broadcast_maximum_fusion
  84.7 0.2 fusion
  84.9 0.1 exponential_add_fusion
  85.0 0.0 collective-permute-done
  85.0 0.0 copy-done.4
  85.1 0.7 pad_maximum_fusion.2
  85.8 0.1 slice.48
  85.9 0.0 copy-done.6
  86.0 0.4 fusion.1
  86.4 0.1 copy.42
  86.5 0.0 collective-permute-done.2
  86.5 0.8 convert_element_type.66
  87.3 0.3 fusion.17
  87.7 0.1 copy.44
  87.8 0.6 broadcast_in_dim.40
  88.4 7.2 %all-to-all-start.1 = ((f32[16,1,128]{2,1,0:T(1,128)}), f32[16,1,128]{2,1,0:T(1,128)S(1)}, u32[]{:S(2)}, u32[]{:S(2)}) async-start(f32[16,1,128]{2,1,0:T(1,128)} %broadcast_in_dim.40), calls=%async_computation.1 | async-start | bytes 16384 | tf_op jit(solution)/shard_map/all_to_all | solution.py:32
  95.7 0.0 reduce-scatter.2.cloned.1.call-start
  95.7 5.2 %all-gather.5.cloned.1.call-done = bf16[256,2048]{1,0:T(8,128)(2,1)} async-done(((bf16[256,128]{1,0:T(8,128)(2,1)}), bf16[256,2048]{1,0:T(8,128)(2,1)}) %all-gather.5.cloned.1.call-update) | async-done | bytes 1048592 | tf_op jit(solution)/shard_map/all_gather | solution.py:21
  100.9 4.8 %fusion.12 = f32[768,2048]{1,0:T(8,128)} fusion(bf16[256,2048]{1,0:T(8,128)(2,1)} %all-gather.5.cloned.1.call-done, bf16[16,8,6,128]{3,2,1,0:T(8,128)(2,1)S(1)} %bitcast.67), kind=kOutput, calls=%fused_computation.25 | convolution fusion | flops 402653184 | bytes 7012352 | tf_op jit(solution)/shard_map/dot_general | solution.py:142
  105.7 0.0 all-to-all-done.1
  105.7 0.1 select_reduce_fusion
  105.8 5.6 %add_convert_fusion = bf16[768,2048]{1,0:T(8,128)(2,1)} fusion(f32[768,2048]{1,0:T(8,128)} %fusion.12, bf16[256,2048]{1,0:T(8,128)(2,1)S(1)} %copy-done.2, s32[]{:T(128)S(6)} %select_n.38, f32[896,128]{1,0:T(8,128)S(1)} %bitcast.65, f32[768,128]{1,0:T(8,128)S(1)} %slice_subtract_fusion, f32[128]{0:T(128)S(1)} %copy-done.10, f32[768]{0:T(1024)S(1)} %get-tuple-element.9, ...), kind=kOutput, calls=%fused_computation | convolution fusion | flops 406683648 | bytes 11412485 | tf_op jit(solution)/shard_map/dot_general | solution.py:143
  111.4 0.0 reduce-scatter.2.cloned.1.call-update
  111.4 35.3 %reduce-scatter.2.cloned.1.call-done = bf16[96,2048]{1,0:T(8,128)(2,1)} async-done(((bf16[768,2048]{1,0:T(8,128)(2,1)}), bf16[96,2048]{1,0:T(8,128)(2,1)}) %reduce-scatter.2.cloned.1.call-update) | async-done | bytes 393232 | tf_op jit(solution)/shard_map/reduce_scatter | solution.py:140
  (28 shorter events, 0.2 us)
Async XLA Ops:
  6.5 50.7 %all-gather.3.cloned.1.call-start = ((), (), s32[]{:S(2)}) async-start(), calls=%async_computation.3 | async-start | bytes 1671168 | tf_op jit(solution)/shard_map/all_gather | solution.py:21
  14.1 4.8 %copy-start.7 = (bf16[128,128]{1,0:T(8,128)(2,1)S(1)}, bf16[128,128]{1,0:T(8,128)(2,1)}, u32[]{:S(2)}) copy-start(bf16[128,128]{1,0:T(8,128)(2,1)} %param.19) | copy-start | bytes 98308
  14.1 4.8 %copy-start.8 = (bf16[128,128]{1,0:T(8,128)(2,1)S(1)}, bf16[128,128]{1,0:T(8,128)(2,1)}, u32[]{:S(2)}) copy-start(bf16[128,128]{1,0:T(8,128)(2,1)} %param.18) | copy-start | bytes 98308
  14.1 43.1 %all-to-all-start = ((bf16[8,96,2048]{2,1,0:T(8,128)(2,1)}), bf16[8,96,2048]{2,1,0:T(8,128)(2,1)S(1)}, u32[]{:S(2)}, u32[]{:S(2)}) async-start(bf16[8,96,2048]{2,1,0:T(8,128)(2,1)} %stack.2), calls=%async_computation | async-start | bytes 6291456 | tf_op jit(solution)/shard_map/all_to_all | solution.py:61
  18.9 82.0 %all-gather.5.cloned.1.call-start = ((), (), s32[]{:S(2)}) async-start(), calls=%async_computation.4 | async-start | bytes 1114112 | tf_op jit(solution)/shard_map/all_gather | solution.py:21
  59.4 0.7 copy-start.5
  62.4 8.8 %copy-start.3 = (bf16[768,64]{0,1:T(8,128)(2,1)}, bf16[768,64]{0,1:T(8,128)(2,1)S(1)}, u32[]{:S(2)}) copy-start(bf16[768,64]{0,1:T(8,128)(2,1)S(1)} %convolution_convert_fusion.4) | copy-start | bytes 294916
  63.2 18.9 %collective-permute-start.1 = (bf16[128,64]{0,1:T(8,128)(2,1)}, bf16[128,64]{0,1:T(8,128)(2,1)}, u32[]{:S(2)}, u32[]{:S(2)}) collective-permute-start(bf16[128,64]{0,1:T(8,128)(2,1)} %slice.62), channel_id=1, source_target_pairs={{0,8},{8,16},{16,24},{24,32},{32,40},{40,48},{48,56},{56,64},{64,7... | collective-permute-start | bytes 49160 | tf_op jit(solution)/shard_map/ppermute | solution.py:27
  67.8 17.2 %collective-permute-start = (bf16[128,64]{0,1:T(8,128)(2,1)}, bf16[128,64]{0,1:T(8,128)(2,1)}, u32[]{:S(2)}, u32[]{:S(2)}) collective-permute-start(bf16[128,64]{0,1:T(8,128)(2,1)} %slice.61), channel_id=1, source_target_pairs={{0,8},{8,16},{16,24},{24,32},{32,40},{40,48},{48,56},{56,64},{64,7... | collective-permute-start | bytes 49160 | tf_op jit(solution)/shard_map/ppermute | solution.py:27
  73.8 0.7 copy-start
  75.1 11.4 %collective-permute-start.2 = (bf16[128,128]{1,0:T(8,128)(2,1)}, bf16[128,128]{1,0:T(8,128)(2,1)}, u32[]{:S(2)}, u32[]{:S(2)}) collective-permute-start(bf16[128,128]{1,0:T(8,128)(2,1)} %slice.63), channel_id=1, source_target_pairs={{0,8},{8,16},{16,24},{24,32},{32,40},{40,48},{48,56},{56,64},{64,7... | collective-permute-start | bytes 98312 | tf_op jit(solution)/shard_map/ppermute | solution.py:27
  83.0 1.7 %copy-start.9 = (f32[2]{0:T(128)S(1)}, f32[2]{0:T(128)}, u32[]{:S(2)}) copy-start(f32[2]{0:T(128)} %param.16) | copy-start | bytes 28
  83.1 1.9 %copy-start.4 = (bf16[768,64]{0,1:T(8,128)(2,1)S(1)}, bf16[768,64]{0,1:T(8,128)(2,1)}, u32[]{:S(2)}) copy-start(bf16[768,64]{0,1:T(8,128)(2,1)} %copy-done.3) | copy-start | bytes 294916
  84.6 1.3 copy-start.6
  88.4 17.3 %all-to-all-start.1 = ((f32[16,1,128]{2,1,0:T(1,128)}), f32[16,1,128]{2,1,0:T(1,128)S(1)}, u32[]{:S(2)}, u32[]{:S(2)}) async-start(f32[16,1,128]{2,1,0:T(1,128)} %broadcast_in_dim.40), calls=%async_computation.1 | async-start | bytes 16384 | tf_op jit(solution)/shard_map/all_to_all | solution.py:32
  95.7 51.1 %reduce-scatter.2.cloned.1.call-start = ((), (), s32[]{:S(2)}) async-start(), calls=%async_computation.5 | async-start | bytes 3538944 | tf_op jit(solution)/shard_map/reduce_scatter | solution.py:140
  100.9 4.9 %copy-start.1 = (bf16[768,128]{1,0:T(8,128)(2,1)S(1)}, bf16[768,128]{1,0:T(8,128)(2,1)}, u32[]{:S(2)}) copy-start(bf16[768,128]{1,0:T(8,128)(2,1)} %copy-done) | copy-start | bytes 589828
  100.9 4.9 %copy-start.2 = (bf16[256,2048]{1,0:T(8,128)(2,1)S(1)}, bf16[256,2048]{1,0:T(8,128)(2,1)}, u32[]{:S(2)}) copy-start(bf16[256,2048]{1,0:T(8,128)(2,1)} %all-gather.5.cloned.1.call-done) | copy-start | bytes 3145732
  100.9 4.9 %copy-start.10 = (f32[128]{0:T(128)S(1)}, f32[128]{0:T(128)}, u32[]{:S(2)}) copy-start(f32[128]{0:T(128)} %param.17) | copy-start | bytes 1540
Sparse Core Ops, SparseCore 0:
  9.9 46.2 all-gather.2
  58.3 42.5 all-gather.4
  111.5 35.1 reduce-scatter.1
